TPU v7x, 32 devices: a whole 2x2x4 slice. The times are simulated.
32 devices in a mesh: sp: 16 (over z, y, x), tp: 2 (over core).
Axes of the slice: x: 2, y: 2, z: 4, core: 2. Of those that a mesh axis runs over, the one named last changes fastest.
Arguments:
- mixer_in: bfloat16 [8192, 1024], P('sp', 'tp'), may hold values from -6 to 6
- residual: bfloat16 [8192, 2048], P(('sp', 'tp')), may hold values from -6 to 6
- decay_real: float32 [64, 64], P('tp'), may hold values from -2 to 0, as said below
- decay_imag: float32 [64, 64], P('tp'), may hold values from 1 to 200
- log_step: float32 [64], P('tp'), may hold values from -3.9 to -2.5
- in_real: float32 [64, 64, 16], P('tp'), may hold values from -1 to 1
- in_imag: float32 [64, 64, 16], P('tp'), may hold values from -1 to 1
- output_real: float32 [64, 16, 64], P('tp'), may hold values from -0.5 to 0.5
- output_imaginary: float32 [64, 16, 64], P('tp'), may hold values from -0.5 to 0.5
- skip: float32 [1024], P('tp'), may hold values from -4 to 4
- out_proj: bfloat16 [1024, 2048], P('tp'), may hold values from -0.1875 to 0.1875
- norm_gain: float32 [2048], replicated, may hold values from 0.1 to 1.9
- w_gate: bfloat16 [2048, 5632], P('sp', 'tp'), may hold values from -0.125 to 0.125
- w_up: bfloat16 [2048, 5632], P('sp', 'tp'), may hold values from -0.125 to 0.125
- w_down: bfloat16 [5632, 2048], P('tp', 'sp'), may hold values from -0.078125 to 0.078125
Outputs:
- output: bfloat16 [8192, 2048], P(('sp', 'tp'))
Inputs may be any that keep to these rules, and one draw needn't show every extreme that they name: `decay_real`: every entry is negative.
All inputs are finite; a program needn't handle non-finite values.
Results may differ from a plain program's by a relative error of at most 0.02.
Values may be sent and summed in bfloat16 or wider, within the bound.
A program may use at most 128 MiB of HBM per device.

v0:
```python
import jax
import jax.numpy as jnp
from jax import lax
from jax.sharding import PartitionSpec as P


def prefix(value, axis, join, neutral):
    count, mine = (lax.axis_size(axis), lax.axis_index(axis))
    pieces = jax.tree.map(lambda part: lax.all_gather(part, axis), value)
    subtotal = jax.tree.map(
        lambda part, zero: jnp.full_like(part, 0) + jnp.asarray(zero, part.dtype), value, neutral
    )

    def step(position, subtotal):
        longer = join(subtotal, jax.tree.map(lambda part: part[position], pieces))
        return jax.tree.map(lambda new, old: jnp.where(position < mine, new, old), longer, subtotal)

    return lax.fori_loop(0, count - 1, step, subtotal)


def discrete(decay_real, decay_imag, log_step, in_real, in_imag):
    step_size = jnp.exp(log_step)[:, None]
    magnitude = jnp.exp(decay_real * step_size)
    angle = decay_imag * step_size
    power_re = magnitude * jnp.cos(angle)
    power_im = magnitude * jnp.sin(angle)
    denom = decay_real * decay_real + decay_imag * decay_imag
    ratio_re = ((power_re - 1.0) * decay_real + power_im * decay_imag) / denom
    ratio_im = (power_im * decay_real - (power_re - 1.0) * decay_imag) / denom
    drive_re = ratio_re[..., None] * in_real - ratio_im[..., None] * in_imag
    drive_im = ratio_re[..., None] * in_imag + ratio_im[..., None] * in_real
    return (power_re, power_im, drive_re, drive_im)


def combine(earlier, later):
    ar1, ai1, br1, bi1 = earlier
    ar2, ai2, br2, bi2 = later
    return (
        ar2 * ar1 - ai2 * ai1,
        ar2 * ai1 + ai2 * ar1,
        ar2 * br1 - ai2 * bi1 + br2,
        ar2 * bi1 + ai2 * br1 + bi2,
    )


def spread_blocks(matrix):
    groups = matrix.shape[0]
    unit_blocks = jnp.eye(groups, dtype=jnp.float32)[:, None, :, None]
    turned = jnp.transpose(matrix, (0, 2, 1))[:, :, None, :]
    return (unit_blocks * turned).reshape(groups * matrix.shape[2], groups * matrix.shape[1])


def local_states(power_re, power_im, drive_re, drive_im):
    rows, flat_size = drive_re.shape
    span = 8
    blocks = rows // span
    dr = drive_re.reshape(blocks, span, flat_size)
    di = drive_im.reshape(blocks, span, flat_size)
    cur_re = dr[:, 0]
    cur_im = di[:, 0]
    inner_re = [cur_re]
    inner_im = [cur_im]
    lift_re = [power_re]
    lift_im = [power_im]
    for index in range(1, span):
        cur_re, cur_im = (
            power_re * cur_re - power_im * cur_im + dr[:, index],
            power_re * cur_im + power_im * cur_re + di[:, index],
        )
        inner_re.append(cur_re)
        inner_im.append(cur_im)
        prev_re, prev_im = (lift_re[-1], lift_im[-1])
        lift_re.append(power_re * prev_re - power_im * prev_im)
        lift_im.append(power_re * prev_im + power_im * prev_re)
    inner_re = jnp.stack(inner_re, axis=1)
    inner_im = jnp.stack(inner_im, axis=1)
    lift_re = jnp.concatenate(lift_re, axis=0)[None]
    lift_im = jnp.concatenate(lift_im, axis=0)[None]
    block_re = jnp.broadcast_to(lift_re[0, span - 1][None], (blocks, flat_size))
    block_im = jnp.broadcast_to(lift_im[0, span - 1][None], (blocks, flat_size))
    totals = (block_re, block_im, cur_re, cur_im)
    distance = 1
    while distance < blocks:
        ones = jnp.ones((distance, flat_size), jnp.float32)
        zeros = jnp.zeros((distance, flat_size), jnp.float32)
        moved = (
            jnp.concatenate([ones, totals[0][:-distance]], axis=0),
            jnp.concatenate([zeros, totals[1][:-distance]], axis=0),
            jnp.concatenate([zeros, totals[2][:-distance]], axis=0),
            jnp.concatenate([zeros, totals[3][:-distance]], axis=0),
        )
        totals = combine(moved, totals)
        distance = distance * 2
    one_row = jnp.ones((1, flat_size), jnp.float32)
    zero_row = jnp.zeros((1, flat_size), jnp.float32)
    before_a_re = jnp.concatenate([one_row, totals[0][:-1]], axis=0)[:, None]
    before_a_im = jnp.concatenate([zero_row, totals[1][:-1]], axis=0)[:, None]
    before_re = jnp.concatenate([zero_row, totals[2][:-1]], axis=0)[:, None]
    before_im = jnp.concatenate([zero_row, totals[3][:-1]], axis=0)[:, None]
    state_real = inner_re + lift_re * before_re - lift_im * before_im
    state_imaginary = inner_im + lift_re * before_im + lift_im * before_re
    pw_re = lift_re * before_a_re - lift_im * before_a_im
    pw_im = lift_re * before_a_im + lift_im * before_a_re
    summary = (totals[0][-1], totals[1][-1], totals[2][-1], totals[3][-1])
    return (
        pw_re.reshape(rows, flat_size),
        pw_im.reshape(rows, flat_size),
        state_real.reshape(rows, flat_size),
        state_imaginary.reshape(rows, flat_size),
        summary,
    )


def on_device(
    mixer_in,
    residual,
    decay_real,
    decay_imag,
    log_step,
    in_real,
    in_imag,
    output_real,
    output_imaginary,
    skip,
    out_proj,
    norm_gain,
    w_gate,
    w_up,
    w_down,
):
    highest_precision = lax.Precision.HIGHEST
    power_re, power_im, bar_re, bar_im = discrete(
        decay_real, decay_imag, log_step, in_real, in_imag
    )
    flat_size = decay_real.shape[0] * decay_real.shape[1]
    read_in = jnp.concatenate([spread_blocks(bar_re), spread_blocks(bar_im)], axis=1)
    signal = mixer_in.astype(jnp.float32)
    drive = jnp.dot(signal, read_in, precision=highest_precision)
    drive_re = drive[:, :flat_size]
    drive_im = drive[:, flat_size:]
    pw_re, pw_im, state_real, state_imaginary, summary = local_states(
        power_re.reshape(1, flat_size), power_im.reshape(1, flat_size), drive_re, drive_im
    )
    zero_line = jnp.zeros((flat_size,), jnp.float32)
    identity = (jnp.ones((flat_size,), jnp.float32), zero_line, zero_line, zero_line)
    _, _, hold_re, hold_im = prefix(summary, "sp", combine, identity)
    state_real = state_real + pw_re * hold_re[None] - pw_im * hold_im[None]
    state_imaginary = state_imaginary + pw_re * hold_im[None] + pw_im * hold_re[None]
    read_out = jnp.concatenate(
        [spread_blocks(output_real), -spread_blocks(output_imaginary)], axis=0
    )
    mixed_before_norm = jnp.dot(
        jnp.concatenate([state_real, state_imaginary], axis=1),
        read_out,
        precision=highest_precision,
    )
    mixed_before_norm = mixed_before_norm + skip[None] * signal
    activated = jax.nn.gelu(mixed_before_norm).astype(jnp.bfloat16)
    partial_value = jnp.dot(activated, out_proj, preferred_element_type=jnp.float32).astype(
        jnp.bfloat16
    )
    mixed = lax.psum_scatter(
        lax.optimization_barrier(partial_value).astype(jnp.float32).astype(jnp.bfloat16),
        "tp",
        scatter_dimension=0,
        tiled=True,
    )
    carried = residual.astype(jnp.float32) + mixed.astype(jnp.float32)
    scale = lax.rsqrt(jnp.mean(carried * carried, axis=-1, keepdims=True) + 1e-06)
    normed = (carried * scale * norm_gain).astype(jnp.bfloat16)
    full_rows = lax.all_gather(normed, "tp", axis=0, tiled=True)
    gate = jnp.dot(
        full_rows,
        lax.all_gather(w_gate, "sp", axis=0, tiled=True),
        preferred_element_type=jnp.float32,
    )
    up = jnp.dot(
        full_rows,
        lax.all_gather(w_up, "sp", axis=0, tiled=True),
        preferred_element_type=jnp.float32,
    )
    down_columns = lax.all_gather(w_down, "sp", axis=1, tiled=True)
    hidden = (jax.nn.silu(gate) * up).astype(jnp.bfloat16)
    partial_value = jnp.dot(hidden, down_columns, preferred_element_type=jnp.float32).astype(
        jnp.bfloat16
    )
    down = lax.psum_scatter(
        lax.optimization_barrier(partial_value).astype(jnp.float32).astype(jnp.bfloat16),
        "tp",
        scatter_dimension=0,
        tiled=True,
    )
    return (carried + 0.5 * down.astype(jnp.float32)).astype(jnp.bfloat16)


def solution(mesh):
    return jax.shard_map(
        on_device,
        mesh=mesh,
        in_specs=(
            P("sp", "tp"),
            P(("sp", "tp"), None),
            P("tp", None),
            P("tp", None),
            P("tp"),
            P("tp", None, None),
            P("tp", None, None),
            P("tp", None, None),
            P("tp", None, None),
            P("tp"),
            P("tp", None),
            P(),
            P("sp", "tp"),
            P("sp", "tp"),
            P("tp", "sp"),
        ),
        out_specs=P(("sp", "tp"), None),
        check_vma=False,
    )
```

profile of v0, /device:TPU:0, one launch (start us, length us, event | category | flops | bytes accessed | tf_op | source)
XLA Modules:
  0.0 897.7 jit_solution(369592521946466958)
XLA Ops:
  7.4 0.9 cosine_multiply_fusion
  8.6 1.1 subtract_bitcast_fusion
  9.7 8.3 broadcast_multiply_fusion.2
  18.1 7.8 mul.1865
  25.9 7.9 mul.1870
  33.8 10.5 %fusion.11 = f32[512,4096]{1,0:T(8,128)S(1)} fusion(bf16[512,512]{1,0:T(8,128)(2,1)S(1)} %copy-done.39, f32[512,2048]{1,0:T(8,128)} %mul.1870, f32[512,2048]{1,0:T(8,128)} %mul.1865), kind=kOutput, calls=%fused_computation.18 | convolution fusion | flops 12886999040 | bytes 17301504 | tf_op jit(solution)/shard_map/dot_general | solution.py:138
  44.2 1.1 slice_bitcast_fusion.1
  45.4 2.5 fusion.61
  47.9 2.7 fusion.62
  50.6 3.0 bitcast_add_fusion.9
  53.6 5.1 multiply_subtract_fusion.3
  58.8 1.4 copy.111
  61.5 6.1 copy_add_fusion.1
  67.6 1.8 bitcast_add_fusion.1
  72.5 1.0 fusion.40
  74.3 0.9 fusion.38
  76.0 2.5 copy.103
  78.5 2.4 copy.106
  80.9 2.4 copy.107
  83.3 2.4 copy.108
  85.8 1.4 copy.109
  87.1 1.3 copy.110
  89.2 43.1 %all-gather.2 = f32[16,1,2048]{2,1,0:T(1,128)S(1)} all-gather(f32[1,1,2048]{2,1,0:T(1,128)S(1)} %slice_bitcast_fusion.3), channel_id=1, replica_groups=mesh['sp'=16,'tp'=2] {'sp'}, dimensions={0}, use_global_device_ids=true | all-gather | bytes 139264 | tf_op jit(solution)/shard_map/all_gather | solution.py:9
  132.3 36.1 %all-gather.1 = f32[16,1,2048]{2,1,0:T(1,128)S(1)} all-gather(f32[1,1,2048]{2,1,0:T(1,128)S(1)} %slice_bitcast_fusion.4), channel_id=1, replica_groups=mesh['sp'=16,'tp'=2] {'sp'}, dimensions={0}, use_global_device_ids=true | all-gather | bytes 139264 | tf_op jit(solution)/shard_map/all_gather | solution.py:9
  168.5 38.2 %all-gather = f32[16,1,2048]{2,1,0:T(1,128)S(1)} all-gather(f32[1,1,2048]{2,1,0:T(1,128)S(1)} %slice_bitcast_fusion.5), channel_id=1, replica_groups=mesh['sp'=16,'tp'=2] {'sp'}, dimensions={0}, use_global_device_ids=true | all-gather | bytes 139264 | tf_op jit(solution)/shard_map/all_gather | solution.py:9
  207.5 36.2 %all-gather.3 = f32[16,1,2048]{2,1,0:T(1,128)S(1)} all-gather(f32[1,1,2048]{2,1,0:T(1,128)S(1)} %slice_bitcast_fusion.2), channel_id=1, replica_groups=mesh['sp'=16,'tp'=2] {'sp'}, dimensions={0}, use_global_device_ids=true | all-gather | bytes 139264 | tf_op jit(solution)/shard_map/all_gather | solution.py:9
  244.3 26.6 %while.16 = (s32[]{:T(128)}, f32[2048]{0:T(1024)S(1)}, f32[2048]{0:T(1024)S(1)}, s32[]{:T(128)}, f32[16,2048]{1,0:T(8,128)}, /*index=5*/f32[16,2048]{1,0:T(8,128...) while((s32[]{:T(128)}, f32[2048]{0:T(1024)S(1)}, f32[2048]{0:T(1024)S(1)}, ...), condition=%wide.region_1.2_spmd.clone, body=%wide.region_0.1_spmd.clone.sunk | while | flops 24580 | bytes 131201 | solution.py:18
  245.4 0.9 constant_dynamic-slice_fusion.7
  247.1 0.9 constant_dynamic-slice_fusion.7
  248.9 0.9 constant_dynamic-slice_fusion.7
  250.7 0.9 constant_dynamic-slice_fusion.7
  254.2 0.9 constant_dynamic-slice_fusion.7
  256.0 0.9 constant_dynamic-slice_fusion.7
  266.5 0.9 constant_dynamic-slice_fusion.7
  268.3 0.9 constant_dynamic-slice_fusion.7
  271.0 2.0 concatenate.124
  273.0 1.9 concatenate.129
  275.0 1.9 concatenate.125
  276.8 2.4 copy.100
  279.2 1.4 copy.101
  280.6 1.3 copy.102
  282.0 1.3 copy.98
  283.3 1.3 copy.99
  284.8 8.1 broadcast_multiply_fusion
  293.0 7.8 mul.2031
  300.8 7.8 neg.11
  308.6 1.9 concatenate.128
  310.5 11.9 %stack.5 = f32[64,8,2048]{2,1,0:T(8,128)} concatenate(f32[64,1,2048]{2,1,0:T(1,128)S(1)} %get-tuple-element.246, f32[64,1,2048]{2,1,0:T(1,128)} %copy.106, f32[64,1,2048]{2,1,0:T(1,128)} %copy.107, f32[64,1,2048]{2,1,0:T(1,128)} %copy.108, f32[64,1,2048]{2,1,0:T(1,128)} %copy.109, f32[64,1,2048]{2,1,0:T(1,128)} %copy.110, f32[64,1,2048]{2,1,0:T(1,128)} %copy.111, ...), dimensions={1} | concatenate | bytes 8388608 | tf_op jit(solution)/shard_map/stack | solution.py:76
  322.4 12.0 %stack.4 = f32[64,8,2048]{2,1,0:T(8,128)} concatenate(f32[64,1,2048]{2,1,0:T(1,128)S(1)} %get-tuple-element.248, f32[64,1,2048]{2,1,0:T(1,128)} %copy.98, f32[64,1,2048]{2,1,0:T(1,128)} %copy.99, f32[64,1,2048]{2,1,0:T(1,128)} %copy.100, f32[64,1,2048]{2,1,0:T(1,128)} %copy.101, f32[64,1,2048]{2,1,0:T(1,128)} %copy.102, f32[64,1,2048]{2,1,0:T(1,128)} %copy.103, ...), dimensions={1} | concatenate | bytes 8388608 | tf_op jit(solution)/shard_map/stack | solution.py:75
  334.4 7.0 fusion.15
  341.4 0.9 copy-done.22
  342.3 16.5 %fusion.24 = bf16[512,512]{1,0:T(8,128)(2,1)S(1)} fusion(bf16[512,512]{1,0:T(8,128)(2,1)S(1)} %copy-done.40, f32[2048,512]{0,1:T(8,128)S(1)} %copy-done.22, f32[2048,512]{0,1:T(8,128)S(1)} %copy-done.21, f32[512,2048]{1,0:T(8,128)} %get-tuple-element.258, f32[512,2048]{1,0:T(8,128)S(1)} %get-tuple-element.257, f32[512]{0:T(512)S(1)} %copy-done.50), kind=kOutput, calls=%fused_computation.49 | convolution fusion | flops 12892241920 | bytes 17827840 | tf_op jit(solution)/shard_map/dot_general | solution.py:152
  358.8 2.6 convolution_convert_fusion.1
  361.5 7.6 reduce-scatter.3.cloned.1.call-done
  369.1 1.6 multiply_reduce_fusion
  370.8 2.6 multiply_convert_fusion.1
  375.3 10.1 %all-gather.9.cloned.1.call-done = bf16[512,2048]{1,0:T(8,128)(2,1)} async-done(((bf16[256,2048]{1,0:T(8,128)(2,1)}), bf16[512,2048]{1,0:T(8,128)(2,1)}) %all-gather.9.cloned.1.call-update) | async-done | bytes 2097168 | tf_op jit(solution)/shard_map/all_gather | solution.py:171
  385.4 145.4 %all-gather.11.cloned.1.call-done = bf16[2048,2816]{1,0:T(8,128)(2,1)} async-done(((bf16[128,2816]{1,0:T(8,128)(2,1)}), bf16[2048,2816]{1,0:T(8,128)(2,1)}) %all-gather.11.cloned.1.call-update) | async-done | bytes 11534352 | tf_op jit(solution)/shard_map/all_gather | solution.py:174
  530.8 12.7 %fusion.63 = f32[512,2816]{1,0:T(8,128)} fusion(bf16[512,2048]{1,0:T(8,128)(2,1)} %all-gather.9.cloned.1.call-done, bf16[2048,2816]{1,0:T(8,128)(2,1)} %all-gather.11.cloned.1.call-done), kind=kOutput, calls=%fused_computation.183 | convolution fusion | flops 5905580032 | bytes 19398656 | tf_op jit(solution)/shard_map/dot_general | solution.py:172
  543.5 129.6 %all-gather.13.cloned.1.call-done = bf16[2048,2816]{1,0:T(8,128)(2,1)} async-done(((bf16[128,2816]{1,0:T(8,128)(2,1)}), bf16[2048,2816]{1,0:T(8,128)(2,1)}) %all-gather.13.cloned.1.call-update) | async-done | bytes 11534352 | tf_op jit(solution)/shard_map/all_gather | solution.py:179
  673.0 182.8 %all-gather.15.cloned.1.call-done = bf16[2816,2048]{1,0:T(8,128)(2,1)} async-done(((bf16[2816,128]{1,0:T(8,128)(2,1)}), bf16[2816,2048]{1,0:T(8,128)(2,1)}) %all-gather.15.cloned.1.call-update) | async-done | bytes 11534352 | tf_op jit(solution)/shard_map/all_gather | solution.py:182
  855.8 23.4 %convolution_convert_fusion = bf16[512,2048]{1,0:T(8,128)(2,1)} fusion(bf16[2816,2048]{1,0:T(8,128)(2,1)} %all-gather.15.cloned.1.call-done, f32[512,2816]{1,0:T(8,128)} %fusion.63, bf16[512,2048]{1,0:T(8,128)(2,1)} %all-gather.9.cloned.1.call-done, bf16[2048,2816]{1,0:T(8,128)(2,1)} %all-gather.13.cloned.1.call-done), kind=kOutput, calls=%fused_computation.35 | convolution fusion | flops 11820859392 | bytes 33030144 | tf_op jit(solution)/shard_map/dot_general | solution.py:184
  879.2 8.1 reduce-scatter.5.cloned.1.call-done
  887.3 3.1 add_convert_fusion
  (200 shorter events, 30.4 us)
Async XLA Ops:
  6.5 352.3 %copy-start = (bf16[512,2048]{1,0:T(8,128)(2,1)S(1)}, bf16[512,2048]{1,0:T(8,128)(2,1)}, u32[]{:S(2)}) copy-start(bf16[512,2048]{1,0:T(8,128)(2,1)} %param.27) | copy-start | bytes 6291460
  6.5 362.6 %reduce-scatter.3.cloned.1.call-start = ((), (), s32[]{:S(2)}) async-start(), calls=%async_computation.2 | async-start | bytes 3145728 | tf_op jit(solution)/shard_map/reduce_scatter | solution.py:162
  6.5 11.5 %copy-start.47 = (f32[32,32]{0,1:T(8,128)}, f32[32,32]{0,1:T(8,128)S(1)}, u32[]{:S(2)}) copy-start(f32[32,32]{0,1:T(8,128)S(1)} %fusion.52) | copy-start | bytes 12292
  25.9 7.9 copy-start.39
  45.3 5.2 copy-start.1
  45.3 5.2 copy-start.2
  47.8 5.8 copy-start.4
  47.8 5.8 copy-start.12
  47.9 5.8 copy-start.14
  50.6 8.2 copy-start.6
  50.6 8.2 copy-start.16
  50.6 8.2 copy-start.18
  58.8 1.4 copy-start.20
  61.2 8.2 copy-start.41
  61.4 8.1 copy-start.43
  61.4 6.2 copy-start.5
  61.4 6.2 copy-start.7
  61.4 6.2 copy-start.13
  61.4 6.2 copy-start.15
  61.4 6.2 copy-start.17
  61.4 6.2 copy-start.19
  61.5 6.2 copy-start.29
  61.5 6.2 copy-start.30
  73.5 0.8 copy-start.10
  73.5 1.7 copy-start.8
  76.0 9.8 %copy-start.36 = (f32[64,1,2048]{2,0,1:T(8,128)S(1)}, f32[64,1,2048]{2,0,1:T(8,128)}, u32[]{:S(2)}) copy-start(f32[64,1,2048]{2,0,1:T(8,128)} %get-tuple-element.196) | copy-start | bytes 1572868
  76.0 11.2 %copy-start.35 = (f32[64,1,2048]{2,0,1:T(8,128)S(1)}, f32[64,1,2048]{2,0,1:T(8,128)}, u32[]{:S(2)}) copy-start(f32[64,1,2048]{2,0,1:T(8,128)} %get-tuple-element.194) | copy-start | bytes 1572868
  76.0 12.5 %copy-start.24 = (f32[64,2048]{1,0:T(8,128)S(1)}, f32[64,2048]{1,0:T(8,128)}, u32[]{:S(2)}) copy-start(f32[64,2048]{1,0:T(8,128)} %fusion.38) | copy-start | bytes 1572868
  76.0 12.5 %copy-start.23 = (f32[64,2048]{1,0:T(8,128)S(1)}, f32[64,2048]{1,0:T(8,128)}, u32[]{:S(2)}) copy-start(f32[64,2048]{1,0:T(8,128)} %get-tuple-element.206) | copy-start | bytes 1572868
  76.0 12.5 %copy-start.9 = (f32[64,2048]{1,0:T(8,128)S(1)}, f32[64,2048]{1,0:T(8,128)}, u32[]{:S(2)}) copy-start(f32[64,2048]{1,0:T(8,128)} %copy-done.8) | copy-start | bytes 1572868
  76.0 12.5 %copy-start.11 = (f32[64,2048]{1,0:T(8,128)S(1)}, f32[64,2048]{1,0:T(8,128)}, u32[]{:S(2)}) copy-start(f32[64,2048]{1,0:T(8,128)} %copy-done.10) | copy-start | bytes 1572868
  76.0 12.5 %copy-start.38 = (f32[48,2048]{1,0:T(8,128)S(1)}, f32[48,2048]{1,0:T(8,128)}, u32[]{:S(2)}) copy-start(f32[48,2048]{1,0:T(8,128)} %slice.234) | copy-start | bytes 1179652
  88.8 118.6 %copy-start.25 = (f32[64,2048]{1,0:T(8,128)}, f32[64,2048]{1,0:T(8,128)S(1)}, u32[]{:S(2)}) copy-start(f32[64,2048]{1,0:T(8,128)S(1)} %get-tuple-element.203) | copy-start | bytes 1572868
  89.1 118.3 %copy-start.26 = (f32[64,2048]{1,0:T(8,128)}, f32[64,2048]{1,0:T(8,128)S(1)}, u32[]{:S(2)}) copy-start(f32[64,2048]{1,0:T(8,128)S(1)} %get-tuple-element.262) | copy-start | bytes 1572868
  89.1 154.5 %copy-start.27 = (f32[64,2048]{1,0:T(8,128)}, f32[64,2048]{1,0:T(8,128)S(1)}, u32[]{:S(2)}) copy-start(f32[64,2048]{1,0:T(8,128)S(1)} %get-tuple-element.261) | copy-start | bytes 1572868
  89.1 154.5 %copy-start.28 = (f32[64,2048]{1,0:T(8,128)}, f32[64,2048]{1,0:T(8,128)S(1)}, u32[]{:S(2)}) copy-start(f32[64,2048]{1,0:T(8,128)S(1)} %get-tuple-element.267) | copy-start | bytes 1572868
  271.0 8.2 copy-start.34
  271.0 9.6 %copy-start.33 = (f32[64,1,2048]{2,0,1:T(8,128)S(1)}, f32[64,1,2048]{2,0,1:T(8,128)}, u32[]{:S(2)}) copy-start(f32[64,1,2048]{2,0,1:T(8,128)} %get-tuple-element.193) | copy-start | bytes 1572868
  271.0 11.0 %copy-start.32 = (f32[64,1,2048]{2,0,1:T(8,128)S(1)}, f32[64,1,2048]{2,0,1:T(8,128)}, u32[]{:S(2)}) copy-start(f32[64,1,2048]{2,0,1:T(8,128)} %get-tuple-element.201) | copy-start | bytes 1572868
  271.0 12.3 %copy-start.31 = (f32[64,1,2048]{2,0,1:T(8,128)S(1)}, f32[64,1,2048]{2,0,1:T(8,128)}, u32[]{:S(2)}) copy-start(f32[64,1,2048]{2,0,1:T(8,128)} %get-tuple-element.199) | copy-start | bytes 1572868
  271.0 13.6 %copy-start.45 = (f32[32,16,64]{2,1,0:T(8,128)S(1)}, f32[32,16,64]{2,1,0:T(8,128)}, u32[]{:S(2)}) copy-start(f32[32,16,64]{2,1,0:T(8,128)} %param.24) | copy-start | bytes 393220
  273.0 11.7 %copy-start.46 = (f32[32,16,64]{2,1,0:T(8,128)S(1)}, f32[32,16,64]{2,1,0:T(8,128)}, u32[]{:S(2)}) copy-start(f32[32,16,64]{2,1,0:T(8,128)} %param.25) | copy-start | bytes 393220
  273.0 11.8 %copy-start.48 = (f32[32,32]{0,1:T(8,128)S(1)}, f32[32,32]{0,1:T(8,128)}, u32[]{:S(2)}) copy-start(f32[32,32]{0,1:T(8,128)} %copy-done.47) | copy-start | bytes 12292
  322.4 12.0 %copy-start.37 = (f32[64,2048]{1,0:T(8,128)S(1)}, f32[64,2048]{1,0:T(8,128)}, u32[]{:S(2)}) copy-start(f32[64,2048]{1,0:T(8,128)} %concatenate.124) | copy-start | bytes 1572868
  322.4 12.0 %copy-start.42 = (f32[8,2048]{1,0:T(8,128)S(1)}, f32[8,2048]{1,0:T(8,128)}, u32[]{:S(2)}) copy-start(f32[8,2048]{1,0:T(8,128)} %copy-done.41) | copy-start | bytes 196612
  322.4 12.0 %copy-start.44 = (f32[8,2048]{1,0:T(8,128)S(1)}, f32[8,2048]{1,0:T(8,128)}, u32[]{:S(2)}) copy-start(f32[8,2048]{1,0:T(8,128)} %copy-done.43) | copy-start | bytes 196612
  334.3 7.0 copy-start.21
  334.4 7.9 copy-start.22
  334.4 7.9 copy-start.40
  334.4 7.9 copy-start.50
  358.8 10.3 %copy-start.3 = (bf16[256,2048]{1,0:T(8,128)(2,1)S(1)}, bf16[256,2048]{1,0:T(8,128)(2,1)}, u32[]{:S(2)}) copy-start(bf16[256,2048]{1,0:T(8,128)(2,1)} %param.18) | copy-start | bytes 3145732
  361.4 9.3 %copy-start.49 = (f32[2048]{0:T(1024)S(1)}, f32[2048]{0:T(1024)}, u32[]{:S(2)}) copy-start(f32[2048]{0:T(1024)} %param.28) | copy-start | bytes 24580
  361.4 23.9 %all-gather.9.cloned.1.call-start = ((), (), s32[]{:S(2)}) async-start(), calls=%async_computation.3 | async-start | bytes 3145728 | tf_op jit(solution)/shard_map/all_gather | solution.py:171
  373.4 157.4 %all-gather.11.cloned.1.call-start = ((), (), s32[]{:S(2)}) async-start(), calls=%async_computation.4 | async-start | bytes 12255232 | tf_op jit(solution)/shard_map/all_gather | solution.py:174
  374.1 298.9 %all-gather.13.cloned.1.call-start = ((), (), s32[]{:S(2)}) async-start(), calls=%async_computation.5 | async-start | bytes 12255232 | tf_op jit(solution)/shard_map/all_gather | solution.py:179
  374.7 481.1 %all-gather.15.cloned.1.call-start = ((), (), s32[]{:S(2)}) async-start(), calls=%async_computation.6 | async-start | bytes 12255232 | tf_op jit(solution)/shard_map/all_gather | solution.py:182
  375.3 512.1 %reduce-scatter.5.cloned.1.call-start = ((), (), s32[]{:S(2)}) async-start(), calls=%async_computation.7 | async-start | bytes 3145728 | tf_op jit(solution)/shard_map/reduce_scatter | solution.py:187
Sparse Core Ops, SparseCore 0:
  361.6 7.4 reduce-scatter.2
  373.5 11.8 all-gather.8
  388.1 142.5 all-gather.10
  533.4 139.5 all-gather.12
  675.6 180.2 all-gather.14
  879.3 7.9 reduce-scatter.4
where the time goes:
time: 910 us; the launch traced here: 898 us
  waiting for transfers between devices  485 us (53%)
  blocking collectives  154 us (17%)
  local copies, waits for them, and re-layouts  123 us (14%)
  matrix products  65.6 us (7%)
  other arithmetic  54.9 us (6%)
  between operations  14.7 us (2%)
    all_gather x1, waiting for transfers between devices, on_device(): down_columns = lax.all_gather(w_down, 'sp', axis=1, tiled=True)  183 us
    all_gather x4, blocking collectives, prefix(): pieces = jax.tree.map(lambda part: lax.all_gather(part, axis), value)  154 us
    all_gather x1, waiting for transfers between devices, on_device(): lax.all_gather(w_gate, 'sp', axis=0, tiled=True)  145 us
    all_gather x1, waiting for transfers between devices, on_device(): lax.all_gather(w_up, 'sp', axis=0, tiled=True)  130 us
    dynamic_slice x30, local copies, waits for them, and re-layouts, step(): longer = join(subtotal, jax.tree.map(lambda part: part[position], pieces))  25.8 us
    mul x3, local copies, waits for them, and re-layouts, spread_blocks(): unit_blocks * turned  23.5 us
    dot_general x1, matrix products, on_device(): jnp.dot(hidden, down_columns, preferred_element_type=jnp.float32)  23.4 us
  transfers between devices with their start and end apart: 6, of which 6 were waited for; matrix products, arithmetic and copies ran while one was open for 1% of the time, Pallas kernels for 0%

commit v1 on v0

--- a/solution.py
+++ b/solution.py
@@ -2,6 +2,22 @@
 import jax.numpy as jnp
 from jax import lax
 from jax.sharding import PartitionSpec as P
+
+
+def gather_around(x, axis, dim):
+    ways, here, step = (lax.axis_size(axis), lax.axis_index(axis), x.shape[dim])
+    shape = [n * ways if d == dim else n for d, n in enumerate(x.shape)]
+    full = lax.dynamic_update_slice_in_dim(jnp.zeros(shape, x.dtype), x, here * step, axis=dim)
+    going_up = going_down = x
+    for far in range(1, ways // 2 + 1):
+        going_up = lax.ppermute(going_up, axis, [(d, (d + 1) % ways) for d in range(ways)])
+        full = lax.dynamic_update_slice_in_dim(full, going_up, (here - far) % ways * step, axis=dim)
+        if 2 * far < ways:
+            going_down = lax.ppermute(going_down, axis, [(d, (d - 1) % ways) for d in range(ways)])
+            full = lax.dynamic_update_slice_in_dim(
+                full, going_down, (here + far) % ways * step, axis=dim
+            )
+    return full
 
 
 def prefix(value, axis, join, neutral):
@@ -179,7 +195,7 @@
         lax.all_gather(w_up, "sp", axis=0, tiled=True),
         preferred_element_type=jnp.float32,
     )
-    down_columns = lax.all_gather(w_down, "sp", axis=1, tiled=True)
+    down_columns = gather_around(w_down, "sp", 1)
     hidden = (jax.nn.silu(gate) * up).astype(jnp.bfloat16)
     partial_value = jnp.dot(hidden, down_columns, preferred_element_type=jnp.float32).astype(
         jnp.bfloat16

time: 910 us -> 869 us (0.955)
  waiting for transfers between devices: 485 us -> 355 us
  starting transfers between devices: 0.2 us -> 51.3 us
  local copies, waits for them, and re-layouts: 123 us -> 159 us
    ppermute x0 -> x15, waiting for transfers between devices: none -> 230 us  [the longest x8 205 us: gather_around(): lax.ppermute(going_up, axis, [(d, (d + 1) % ways) for d in range(ways)])]
    all_gather x1 -> x0, waiting for transfers between devices: 183 us -> none  [on_device(): down_columns = lax.all_gather(w_down, 'sp', axis=1, tiled=True)]
    all_gather x1, waiting for transfers between devices: 145 us -> 0.01 us  [on_device(): lax.all_gather(w_gate, 'sp', axis=0, tiled=True)]
    ppermute x0 -> x15, starting transfers between devices: none -> 51.1 us  [the longest x7 32.6 us: gather_around(): lax.ppermute(going_down, axis, [(d, (d - 1) % ways) for d in range(ways)])]
    dynamic_update_slice x0 -> x16, local copies, waits for them, and re-layouts: none -> 23.9 us  [the longest x8 12.5 us: gather_around(): lax.dynamic_update_slice_in_dim(full, going_up, (here - far) % ways * ste...]
    all_gather x1, waiting for transfers between devices: 130 us -> 108 us  [on_device(): lax.all_gather(w_up, 'sp', axis=0, tiled=True)]
    all_gather x1, waiting for transfers between devices: 10.1 us -> 0.01 us  [on_device(): full_rows = lax.all_gather(normed, 'tp', axis=0, tiled=True)]
  transfers between devices with their start and end apart: 6 -> 20, of which waited for: 6 -> 14; matrix products, arithmetic and copies ran while one was open for 1% -> 5% of each run, Pallas kernels for 0% -> 0%
where the time goes in v1:
time: 869 us; the launch traced here: 856 us
  waiting for transfers between devices  355 us (41%)
  local copies, waits for them, and re-layouts  159 us (18%)
  blocking collectives  154 us (18%)
  matrix products  65.3 us (8%)
  other arithmetic  57.2 us (7%)
  starting transfers between devices  51.3 us (6%)
  between operations  14.3 us (2%)
    ppermute x8, waiting for transfers between devices, gather_around(): lax.ppermute(going_up, axis, [(d, (d + 1) % ways) for d in range(ways)])  205 us
    all_gather x4, blocking collectives, prefix(): pieces = jax.tree.map(lambda part: lax.all_gather(part, axis), value)  154 us
    all_gather x1, waiting for transfers between devices, on_device(): lax.all_gather(w_up, 'sp', axis=0, tiled=True)  108 us
    ppermute x7, starting transfers between devices, gather_around(): lax.ppermute(going_down, axis, [(d, (d - 1) % ways) for d in range(ways)])  32.6 us
    dynamic_slice x30, local copies, waits for them, and re-layouts, step(): longer = join(subtotal, jax.tree.map(lambda part: part[position], pieces))  26.7 us
    ppermute x7, waiting for transfers between devices, gather_around(): lax.ppermute(going_down, axis, [(d, (d - 1) % ways) for d in range(ways)])  24.6 us
    mul x3, local copies, waits for them, and re-layouts, spread_blocks(): unit_blocks * turned  23.5 us
    dot_general x1, matrix products, on_device(): jnp.dot(hidden, down_columns, preferred_element_type=jnp.float32)  23.3 us
  transfers between devices with their start and end apart: 20, of which 14 were waited for; matrix products, arithmetic and copies ran while one was open for 5% of the time, Pallas kernels for 0%

profile of v1, /device:TPU:0, one launch (start us, length us, event | category | flops | bytes accessed | tf_op | source)
XLA Modules:
  0.0 856.2 jit_solution(8256501099513321165)
XLA Ops:
  9.7 8.3 broadcast_multiply_fusion.2
  18.1 7.8 mul.1913
  25.9 7.9 mul.1918
  33.8 10.5 %fusion.11 = f32[512,4096]{1,0:T(8,128)S(1)} fusion(bf16[512,512]{1,0:T(8,128)(2,1)S(1)} %copy-done.31, f32[512,2048]{1,0:T(8,128)} %mul.1918, f32[512,2048]{1,0:T(8,128)} %mul.1913), kind=kOutput, calls=%fused_computation.18 | convolution fusion | flops 12886999040 | bytes 17301504 | tf_op jit(solution)/shard_map/dot_general | solution.py:154
  45.4 2.5 fusion.61
  47.9 2.7 fusion.62
  50.6 3.0 bitcast_add_fusion.9
  53.7 5.1 multiply_subtract_fusion.3
  61.5 6.0 copy_add_fusion.1
  67.5 4.0 bitcast_add_fusion.1
  77.4 2.5 copy.103
  79.9 2.4 copy.106
  82.3 2.4 copy.107
  84.7 2.4 copy.108
  87.2 2.4 copy.109
  89.5 2.4 copy.110
  92.6 43.2 %all-gather.2 = f32[16,1,2048]{2,1,0:T(1,128)S(1)} all-gather(f32[1,1,2048]{2,1,0:T(1,128)S(1)} %slice_bitcast_fusion.3), channel_id=1, replica_groups=mesh['sp'=16,'tp'=2] {'sp'}, dimensions={0}, use_global_device_ids=true | all-gather | bytes 139264 | tf_op jit(solution)/shard_map/all_gather | solution.py:25
  136.6 36.2 %all-gather.1 = f32[16,1,2048]{2,1,0:T(1,128)S(1)} all-gather(f32[1,1,2048]{2,1,0:T(1,128)S(1)} %slice_bitcast_fusion.4), channel_id=1, replica_groups=mesh['sp'=16,'tp'=2] {'sp'}, dimensions={0}, use_global_device_ids=true | all-gather | bytes 139264 | tf_op jit(solution)/shard_map/all_gather | solution.py:25
  173.5 38.1 %all-gather = f32[16,1,2048]{2,1,0:T(1,128)S(1)} all-gather(f32[1,1,2048]{2,1,0:T(1,128)S(1)} %slice_bitcast_fusion.5), channel_id=1, replica_groups=mesh['sp'=16,'tp'=2] {'sp'}, dimensions={0}, use_global_device_ids=true | all-gather | bytes 139264 | tf_op jit(solution)/shard_map/all_gather | solution.py:25
  212.4 36.3 %all-gather.3 = f32[16,1,2048]{2,1,0:T(1,128)S(1)} all-gather(f32[1,1,2048]{2,1,0:T(1,128)S(1)} %slice_bitcast_fusion.2), channel_id=1, replica_groups=mesh['sp'=16,'tp'=2] {'sp'}, dimensions={0}, use_global_device_ids=true | all-gather | bytes 139264 | tf_op jit(solution)/shard_map/all_gather | solution.py:25
  249.3 27.6 %while.16 = (s32[]{:T(128)}, f32[2048]{0:T(1024)S(1)}, f32[2048]{0:T(1024)S(1)}, s32[]{:T(128)}, f32[16,2048]{1,0:T(8,128)}, /*index=5*/f32[16,2048]{1,0:T(8,128...) while((s32[]{:T(128)}, f32[2048]{0:T(1024)S(1)}, f32[2048]{0:T(1024)S(1)}, ...), condition=%wide.region_1.2_spmd.clone, body=%wide.region_0.1_spmd.clone.sunk | while | flops 24580 | bytes 131201 | solution.py:34
  282.7 2.4 copy.100
  285.1 2.4 copy.101
  287.5 2.4 copy.102
  292.8 8.1 broadcast_multiply_fusion
  300.9 7.8 mul.2079
  308.7 7.8 neg.11
  318.4 11.9 %stack.5 = f32[64,8,2048]{2,1,0:T(8,128)} concatenate(f32[64,1,2048]{2,1,0:T(1,128)S(1)} %get-tuple-element.246, f32[64,1,2048]{2,1,0:T(1,128)} %copy.106, f32[64,1,2048]{2,1,0:T(1,128)} %copy.107, f32[64,1,2048]{2,1,0:T(1,128)} %copy.108, f32[64,1,2048]{2,1,0:T(1,128)} %copy.109, f32[64,1,2048]{2,1,0:T(1,128)} %copy.110, f32[64,1,2048]{2,1,0:T(1,128)} %copy.111, ...), dimensions={1} | concatenate | bytes 8388608 | tf_op jit(solution)/shard_map/stack | solution.py:92
  330.4 12.0 %stack.4 = f32[64,8,2048]{2,1,0:T(8,128)} concatenate(f32[64,1,2048]{2,1,0:T(1,128)S(1)} %get-tuple-element.248, f32[64,1,2048]{2,1,0:T(1,128)} %copy.98, f32[64,1,2048]{2,1,0:T(1,128)} %copy.99, f32[64,1,2048]{2,1,0:T(1,128)} %copy.100, f32[64,1,2048]{2,1,0:T(1,128)} %copy.101, f32[64,1,2048]{2,1,0:T(1,128)} %copy.102, f32[64,1,2048]{2,1,0:T(1,128)} %copy.103, ...), dimensions={1} | concatenate | bytes 8388608 | tf_op jit(solution)/shard_map/stack | solution.py:91
  342.4 7.0 fusion.15
  350.3 16.5 %fusion.24 = bf16[512,512]{1,0:T(8,128)(2,1)S(1)} fusion(bf16[512,512]{1,0:T(8,128)(2,1)S(1)} %copy-done.32, f32[2048,512]{0,1:T(8,128)S(1)} %copy-done.18, f32[2048,512]{0,1:T(8,128)S(1)} %copy-done.17, f32[512,2048]{1,0:T(8,128)} %get-tuple-element.258, f32[512,2048]{1,0:T(8,128)S(1)} %get-tuple-element.257, f32[512]{0:T(512)S(1)} %copy-done.42), kind=kOutput, calls=%fused_computation.49 | convolution fusion | flops 12892241920 | bytes 17827840 | tf_op jit(solution)/shard_map/dot_general | solution.py:168
  366.8 2.6 convolution_convert_fusion.1
  369.5 7.5 reduce-scatter.3.cloned.1.call-done
  378.6 2.6 multiply_convert_fusion.1
  384.5 3.8 collective-permute-start.1
  388.3 32.9 %collective-permute-done = bf16[2816,128]{1,0:T(8,128)(2,1)S(1)} collective-permute-done((bf16[2816,128]{1,0:T(8,128)(2,1)}, bf16[2816,128]{1,0:T(8,128)(2,1)S(1)}, u32[]{:S(2)}, u32[]{:S(2)}) %collective-permute-start) | collective-permute-done | bytes 720928 | tf_op jit(solution)/shard_map/ppermute | solution.py:13
  422.0 2.4 collective-permute-start.2
  424.4 3.2 collective-permute-start.3
  427.6 41.6 %collective-permute-done.2 = bf16[2816,128]{1,0:T(8,128)(2,1)} collective-permute-done((bf16[2816,128]{1,0:T(8,128)(2,1)S(1)}, bf16[2816,128]{1,0:T(8,128)(2,1)}, u32[]{:S(2)}, u32[]{:S(2)}) %collective-permute-start.2) | collective-permute-done | bytes 720928 | tf_op jit(solution)/shard_map/ppermute | solution.py:13
  469.2 2.6 collective-permute-start.4
  471.8 3.5 collective-permute-done.3
  475.3 10.6 %collective-permute-start.5 = (bf16[2816,128]{1,0:T(8,128)(2,1)}, bf16[2816,128]{1,0:T(8,128)(2,1)}, u32[]{:S(2)}, u32[]{:S(2)}) collective-permute-start(bf16[2816,128]{1,0:T(8,128)(2,1)} %collective-permute-done.3), channel_id=1, source_target_pairs={{0,30},{2,0},{4,2},{6,4},{8,6},{10,8},{12,10},{14,12},{16,14},{18,... | collective-permute-start | bytes 2162696 | tf_op jit(solution)/shard_map/ppermute | solution.py:16
  485.9 5.7 broadcast_in_dim.23
  492.6 13.8 %collective-permute-done.4 = bf16[2816,128]{1,0:T(8,128)(2,1)} collective-permute-done((bf16[2816,128]{1,0:T(8,128)(2,1)}, bf16[2816,128]{1,0:T(8,128)(2,1)}, u32[]{:S(2)}, u32[]{:S(2)}) %collective-permute-start.4) | collective-permute-done | bytes 720928 | tf_op jit(solution)/shard_map/ppermute | solution.py:13
  506.3 2.5 collective-permute-start.6
  508.8 2.2 constant_dynamic-update-slice_fusion.14
  511.0 3.1 collective-permute-start.7
  516.2 38.0 %collective-permute-done.6 = bf16[2816,128]{1,0:T(8,128)(2,1)} collective-permute-done((bf16[2816,128]{1,0:T(8,128)(2,1)}, bf16[2816,128]{1,0:T(8,128)(2,1)}, u32[]{:S(2)}, u32[]{:S(2)}) %collective-permute-start.6) | collective-permute-done | bytes 720928 | tf_op jit(solution)/shard_map/ppermute | solution.py:13
  554.2 2.7 collective-permute-start.8
  561.1 3.9 collective-permute-done.7
  567.1 36.6 %collective-permute-done.8 = bf16[2816,128]{1,0:T(8,128)(2,1)S(1)} collective-permute-done((bf16[2816,128]{1,0:T(8,128)(2,1)}, bf16[2816,128]{1,0:T(8,128)(2,1)S(1)}, u32[]{:S(2)}, u32[]{:S(2)}) %collective-permute-start.8) | collective-permute-done | bytes 720928 | tf_op jit(solution)/shard_map/ppermute | solution.py:13
  603.7 2.4 collective-permute-start.10
  606.1 2.2 constant_dynamic-update-slice_fusion.9
  610.3 3.3 collective-permute-done.9
  614.6 30.1 %collective-permute-done.10 = bf16[2816,128]{1,0:T(8,128)(2,1)S(1)} collective-permute-done((bf16[2816,128]{1,0:T(8,128)(2,1)S(1)}, bf16[2816,128]{1,0:T(8,128)(2,1)S(1)}, u32[]{:S(2)}, u32[]{:S(2)}) %collective-permute-start.10) | collective-permute-done | bytes 720928 | tf_op jit(solution)/shard_map/ppermute | solution.py:13
  644.7 2.5 collective-permute-start.12
  649.1 11.8 %collective-permute-start.13 = (bf16[2816,128]{1,0:T(8,128)(2,1)S(1)}, bf16[2816,128]{1,0:T(8,128)(2,1)S(1)}, u32[]{:S(2)}, u32[]{:S(2)}) collective-permute-start(bf16[2816,128]{1,0:T(8,128)(2,1)S(1)} %collective-permute-done.11), channel_id=1, source_target_pairs={{0,30},{2,0},{4,2},{6,4},{8,6},{10,8},{12,10},{14,12},{16,14},{18,... | collective-permute-start | bytes 2162696 | tf_op jit(solution)/shard_map/ppermute | solution.py:16
  665.6 13.9 %collective-permute-done.13 = bf16[2816,128]{1,0:T(8,128)(2,1)S(1)} collective-permute-done((bf16[2816,128]{1,0:T(8,128)(2,1)S(1)}, bf16[2816,128]{1,0:T(8,128)(2,1)S(1)}, u32[]{:S(2)}, u32[]{:S(2)}) %collective-permute-start.13) | collective-permute-done | bytes 720928 | tf_op jit(solution)/shard_map/ppermute | solution.py:16
  680.6 12.3 %collective-permute-done.14 = bf16[2816,128]{1,0:T(8,128)(2,1)S(1)} collective-permute-done((bf16[2816,128]{1,0:T(8,128)(2,1)S(1)}, bf16[2816,128]{1,0:T(8,128)(2,1)S(1)}, u32[]{:S(2)}, u32[]{:S(2)}) %collective-permute-start.14) | collective-permute-done | bytes 720928 | tf_op jit(solution)/shard_map/ppermute | solution.py:13
  694.0 12.5 %fusion.63 = f32[512,2816]{1,0:T(8,128)} fusion(bf16[512,2048]{1,0:T(8,128)(2,1)} %all-gather.8.cloned.1.call-done, bf16[2048,2816]{1,0:T(8,128)(2,1)} %all-gather.10.cloned.1.call-done), kind=kOutput, calls=%fused_computation.199 | convolution fusion | flops 5905580032 | bytes 19398656 | tf_op jit(solution)/shard_map/dot_general | solution.py:188
  706.4 108.3 %all-gather.12.cloned.1.call-done = bf16[2048,2816]{1,0:T(8,128)(2,1)} async-done(((bf16[128,2816]{1,0:T(8,128)(2,1)}), bf16[2048,2816]{1,0:T(8,128)(2,1)}) %all-gather.12.cloned.1.call-update) | async-done | bytes 11534352 | tf_op jit(solution)/shard_map/all_gather | solution.py:195
  814.8 23.3 %convolution_convert_fusion = bf16[512,2048]{1,0:T(8,128)(2,1)} fusion(bf16[2816,2048]{1,0:T(8,128)(2,1)} %constant_dynamic-update-slice_fusion, f32[512,2816]{1,0:T(8,128)} %fusion.63, bf16[512,2048]{1,0:T(8,128)(2,1)} %all-gather.8.cloned.1.call-done, bf16[2048,2816]{1,0:T(8,128)(2,1)} %all-gather.12.cloned.1.call-done), kind=kOutput, calls=%fused_computation.35 | convolution fusion | flops 11820859392 | bytes 33030144 | tf_op jit(solution)/shard_map/dot_general | solution.py:200
  838.1 8.1 reduce-scatter.5.cloned.1.call-done
  846.2 3.1 add_convert_fusion
  (228 shorter events, 81.4 us)
Async XLA Ops:
  6.5 360.3 %copy-start = (bf16[512,2048]{1,0:T(8,128)(2,1)S(1)}, bf16[512,2048]{1,0:T(8,128)(2,1)}, u32[]{:S(2)}) copy-start(bf16[512,2048]{1,0:T(8,128)(2,1)} %param.27) | copy-start | bytes 6291460
  6.5 370.4 %reduce-scatter.3.cloned.1.call-start = ((), (), s32[]{:S(2)}) async-start(), calls=%async_computation.2 | async-start | bytes 3145728 | tf_op jit(solution)/shard_map/reduce_scatter | solution.py:178
  6.5 11.5 %copy-start.39 = (f32[32,32]{0,1:T(8,128)}, f32[32,32]{0,1:T(8,128)S(1)}, u32[]{:S(2)}) copy-start(f32[32,32]{0,1:T(8,128)S(1)} %fusion.52) | copy-start | bytes 12292
  25.9 7.9 copy-start.31
  45.3 5.2 copy-start.1
  45.3 5.2 copy-start.2
  47.8 5.8 copy-start.4
  47.9 5.8 copy-start.12
  47.9 5.8 copy-start.13
  50.6 8.2 copy-start.6
  50.6 8.2 copy-start.14
  50.6 8.2 copy-start.15
  58.8 1.4 copy-start.16
  61.3 10.9 %copy-start.33 = (f32[8,2048]{1,0:T(8,128)}, f32[8,2048]{1,0:T(8,128)S(1)}, u32[]{:S(2)}) copy-start(f32[8,2048]{1,0:T(8,128)S(1)} %concatenate.100) | copy-start | bytes 196612
  61.4 10.8 %copy-start.35 = (f32[8,2048]{1,0:T(8,128)}, f32[8,2048]{1,0:T(8,128)S(1)}, u32[]{:S(2)}) copy-start(f32[8,2048]{1,0:T(8,128)S(1)} %concatenate.102) | copy-start | bytes 196612
  61.4 10.0 %copy-start.5 = (f32[64,1,2048]{2,1,0:T(1,128)S(1)}, f32[64,1,2048]{2,1,0:T(1,128)}, u32[]{:S(2)}) copy-start(f32[64,1,2048]{2,1,0:T(1,128)} %copy-done.4) | copy-start | bytes 1572868
  61.4 10.0 %copy-start.7 = (f32[64,1,2048]{2,1,0:T(1,128)S(1)}, f32[64,1,2048]{2,1,0:T(1,128)}, u32[]{:S(2)}) copy-start(f32[64,1,2048]{2,1,0:T(1,128)} %copy-done.6) | copy-start | bytes 1572868
  75.5 1.1 copy-start.8
  75.5 1.9 copy-start.10
  77.3 14.6 %copy-start.20 = (f32[64,2048]{1,0:T(8,128)S(1)}, f32[64,2048]{1,0:T(8,128)}, u32[]{:S(2)}) copy-start(f32[64,2048]{1,0:T(8,128)} %fusion.38) | copy-start | bytes 1572868
  77.4 14.6 %copy-start.19 = (f32[64,2048]{1,0:T(8,128)S(1)}, f32[64,2048]{1,0:T(8,128)}, u32[]{:S(2)}) copy-start(f32[64,2048]{1,0:T(8,128)} %get-tuple-element.206) | copy-start | bytes 1572868
  77.4 14.6 %copy-start.9 = (f32[64,2048]{1,0:T(8,128)S(1)}, f32[64,2048]{1,0:T(8,128)}, u32[]{:S(2)}) copy-start(f32[64,2048]{1,0:T(8,128)} %copy-done.8) | copy-start | bytes 1572868
  77.4 14.6 %copy-start.11 = (f32[64,2048]{1,0:T(8,128)S(1)}, f32[64,2048]{1,0:T(8,128)}, u32[]{:S(2)}) copy-start(f32[64,2048]{1,0:T(8,128)} %copy-done.10) | copy-start | bytes 1572868
  77.4 14.6 %copy-start.28 = (f32[48,2048]{1,0:T(8,128)S(1)}, f32[48,2048]{1,0:T(8,128)}, u32[]{:S(2)}) copy-start(f32[48,2048]{1,0:T(8,128)} %slice.234) | copy-start | bytes 1179652
  92.3 120.1 %copy-start.21 = (f32[64,2048]{1,0:T(8,128)}, f32[64,2048]{1,0:T(8,128)S(1)}, u32[]{:S(2)}) copy-start(f32[64,2048]{1,0:T(8,128)S(1)} %get-tuple-element.203) | copy-start | bytes 1572868
  92.6 119.8 %copy-start.22 = (f32[64,2048]{1,0:T(8,128)}, f32[64,2048]{1,0:T(8,128)S(1)}, u32[]{:S(2)}) copy-start(f32[64,2048]{1,0:T(8,128)S(1)} %get-tuple-element.262) | copy-start | bytes 1572868
  92.6 156.1 %copy-start.23 = (f32[64,2048]{1,0:T(8,128)}, f32[64,2048]{1,0:T(8,128)S(1)}, u32[]{:S(2)}) copy-start(f32[64,2048]{1,0:T(8,128)S(1)} %get-tuple-element.261) | copy-start | bytes 1572868
  92.6 156.1 %copy-start.24 = (f32[64,2048]{1,0:T(8,128)}, f32[64,2048]{1,0:T(8,128)S(1)}, u32[]{:S(2)}) copy-start(f32[64,2048]{1,0:T(8,128)S(1)} %get-tuple-element.267) | copy-start | bytes 1572868
  92.6 200.0 %copy-start.37 = (f32[32,16,64]{2,1,0:T(8,128)S(1)}, f32[32,16,64]{2,1,0:T(8,128)}, u32[]{:S(2)}) copy-start(f32[32,16,64]{2,1,0:T(8,128)} %param.24) | copy-start | bytes 393220
  172.8 120.0 %copy-start.40 = (f32[32,32]{0,1:T(8,128)S(1)}, f32[32,32]{0,1:T(8,128)}, u32[]{:S(2)}) copy-start(f32[32,32]{0,1:T(8,128)} %copy-done.39) | copy-start | bytes 12292
  276.9 13.0 %copy-start.26 = (f32[64,1,2048]{2,0,1:T(8,128)S(1)}, f32[64,1,2048]{2,0,1:T(8,128)}, u32[]{:S(2)}) copy-start(f32[64,1,2048]{2,0,1:T(8,128)} %get-tuple-element.201) | copy-start | bytes 1572868
  276.9 14.3 %copy-start.25 = (f32[64,1,2048]{2,0,1:T(8,128)S(1)}, f32[64,1,2048]{2,0,1:T(8,128)}, u32[]{:S(2)}) copy-start(f32[64,1,2048]{2,0,1:T(8,128)} %get-tuple-element.199) | copy-start | bytes 1572868
  276.9 15.7 %copy-start.38 = (f32[32,16,64]{2,1,0:T(8,128)S(1)}, f32[32,16,64]{2,1,0:T(8,128)}, u32[]{:S(2)}) copy-start(f32[32,16,64]{2,1,0:T(8,128)} %param.25) | copy-start | bytes 393220
  330.3 12.0 %copy-start.27 = (f32[64,2048]{1,0:T(8,128)S(1)}, f32[64,2048]{1,0:T(8,128)}, u32[]{:S(2)}) copy-start(f32[64,2048]{1,0:T(8,128)} %concatenate.124) | copy-start | bytes 1572868
  330.3 12.0 %copy-start.34 = (f32[8,2048]{1,0:T(8,128)S(1)}, f32[8,2048]{1,0:T(8,128)}, u32[]{:S(2)}) copy-start(f32[8,2048]{1,0:T(8,128)} %copy-done.33) | copy-start | bytes 196612
  330.3 12.0 %copy-start.36 = (f32[8,2048]{1,0:T(8,128)S(1)}, f32[8,2048]{1,0:T(8,128)}, u32[]{:S(2)}) copy-start(f32[8,2048]{1,0:T(8,128)} %copy-done.35) | copy-start | bytes 196612
  342.3 7.0 copy-start.17
  342.4 7.9 copy-start.18
  342.4 7.9 copy-start.32
  342.4 7.9 copy-start.42
  366.8 10.2 %copy-start.3 = (bf16[256,2048]{1,0:T(8,128)(2,1)S(1)}, bf16[256,2048]{1,0:T(8,128)(2,1)}, u32[]{:S(2)}) copy-start(bf16[256,2048]{1,0:T(8,128)(2,1)} %param.18) | copy-start | bytes 3145732
  366.8 11.8 %copy-start.41 = (f32[2048]{0:T(1024)S(1)}, f32[2048]{0:T(1024)}, u32[]{:S(2)}) copy-start(f32[2048]{0:T(1024)} %param.28) | copy-start | bytes 24580
  369.4 324.5 %all-gather.8.cloned.1.call-start = ((), (), s32[]{:S(2)}) async-start(), calls=%async_computation.3 | async-start | bytes 3145728 | tf_op jit(solution)/shard_map/all_gather | solution.py:187
  381.3 312.7 %all-gather.10.cloned.1.call-start = ((), (), s32[]{:S(2)}) async-start(), calls=%async_computation.4 | async-start | bytes 12255232 | tf_op jit(solution)/shard_map/all_gather | solution.py:190
  382.0 432.8 %all-gather.12.cloned.1.call-start = ((), (), s32[]{:S(2)}) async-start(), calls=%async_computation.5 | async-start | bytes 12255232 | tf_op jit(solution)/shard_map/all_gather | solution.py:195
  382.6 463.6 %reduce-scatter.5.cloned.1.call-start = ((), (), s32[]{:S(2)}) async-start(), calls=%async_computation.6 | async-start | bytes 3145728 | tf_op jit(solution)/shard_map/reduce_scatter | solution.py:203
  382.6 38.5 %collective-permute-start = (bf16[2816,128]{1,0:T(8,128)(2,1)}, bf16[2816,128]{1,0:T(8,128)(2,1)S(1)}, u32[]{:S(2)}, u32[]{:S(2)}) collective-permute-start(bf16[2816,128]{1,0:T(8,128)(2,1)} %param.31), channel_id=1, source_target_pairs={{0,2},{2,4},{4,6},{6,8},{8,10},{10,12},{12,14},{14,16},{16,18},{18... | collective-permute-start | bytes 2162696 | tf_op jit(solution)/shard_map/ppermute | solution.py:13
  384.5 39.9 %collective-permute-start.1 = (bf16[2816,128]{1,0:T(8,128)(2,1)}, bf16[2816,128]{1,0:T(8,128)(2,1)}, u32[]{:S(2)}, u32[]{:S(2)}) collective-permute-start(bf16[2816,128]{1,0:T(8,128)(2,1)} %param.31), channel_id=1, source_target_pairs={{0,30},{2,0},{4,2},{6,4},{8,6},{10,8},{12,10},{14,12},{16,14},{18,... | collective-permute-start | bytes 2162696 | tf_op jit(solution)/shard_map/ppermute | solution.py:16
  421.2 0.9 copy-start.30
  422.0 47.2 %collective-permute-start.2 = (bf16[2816,128]{1,0:T(8,128)(2,1)S(1)}, bf16[2816,128]{1,0:T(8,128)(2,1)}, u32[]{:S(2)}, u32[]{:S(2)}) collective-permute-start(bf16[2816,128]{1,0:T(8,128)(2,1)S(1)} %collective-permute-done), channel_id=1, source_target_pairs={{0,2},{2,4},{4,6},{6,8},{8,10},{10,12},{12,14},{14,16},{16,18},{18... | collective-permute-start | bytes 2162696 | tf_op jit(solution)/shard_map/ppermute | solution.py:13
  424.4 50.9 %collective-permute-start.3 = (bf16[2816,128]{1,0:T(8,128)(2,1)}, bf16[2816,128]{1,0:T(8,128)(2,1)}, u32[]{:S(2)}, u32[]{:S(2)}) collective-permute-start(bf16[2816,128]{1,0:T(8,128)(2,1)} %collective-permute-done.1), channel_id=1, source_target_pairs={{0,30},{2,0},{4,2},{6,4},{8,6},{10,8},{12,10},{14,12},{16,14},{18,... | collective-permute-start | bytes 2162696 | tf_op jit(solution)/shard_map/ppermute | solution.py:16
  469.2 37.1 %collective-permute-start.4 = (bf16[2816,128]{1,0:T(8,128)(2,1)}, bf16[2816,128]{1,0:T(8,128)(2,1)}, u32[]{:S(2)}, u32[]{:S(2)}) collective-permute-start(bf16[2816,128]{1,0:T(8,128)(2,1)} %collective-permute-done.2), channel_id=1, source_target_pairs={{0,2},{2,4},{4,6},{6,8},{8,10},{10,12},{12,14},{14,16},{16,18},{18... | collective-permute-start | bytes 2162696 | tf_op jit(solution)/shard_map/ppermute | solution.py:13
  471.8 19.8 %copy-start.29 = (bf16[2816,128]{1,0:T(8,128)(2,1)S(1)}, bf16[2816,128]{1,0:T(8,128)(2,1)}, u32[]{:S(2)}) copy-start(bf16[2816,128]{1,0:T(8,128)(2,1)} %param.31) | copy-start | bytes 2162692
  475.3 35.7 %collective-permute-start.5 = (bf16[2816,128]{1,0:T(8,128)(2,1)}, bf16[2816,128]{1,0:T(8,128)(2,1)}, u32[]{:S(2)}, u32[]{:S(2)}) collective-permute-start(bf16[2816,128]{1,0:T(8,128)(2,1)} %collective-permute-done.3), channel_id=1, source_target_pairs={{0,30},{2,0},{4,2},{6,4},{8,6},{10,8},{12,10},{14,12},{16,14},{18,... | collective-permute-start | bytes 2162696 | tf_op jit(solution)/shard_map/ppermute | solution.py:16
  506.3 47.8 %collective-permute-start.6 = (bf16[2816,128]{1,0:T(8,128)(2,1)}, bf16[2816,128]{1,0:T(8,128)(2,1)}, u32[]{:S(2)}, u32[]{:S(2)}) collective-permute-start(bf16[2816,128]{1,0:T(8,128)(2,1)} %collective-permute-done.4), channel_id=1, source_target_pairs={{0,2},{2,4},{4,6},{6,8},{8,10},{10,12},{12,14},{14,16},{16,18},{18... | collective-permute-start | bytes 2162696 | tf_op jit(solution)/shard_map/ppermute | solution.py:13
  511.0 54.0 %collective-permute-start.7 = (bf16[2816,128]{1,0:T(8,128)(2,1)}, bf16[2816,128]{1,0:T(8,128)(2,1)S(1)}, u32[]{:S(2)}, u32[]{:S(2)}) collective-permute-start(bf16[2816,128]{1,0:T(8,128)(2,1)} %collective-permute-done.5), channel_id=1, source_target_pairs={{0,30},{2,0},{4,2},{6,4},{8,6},{10,8},{12,10},{14,12},{16,14},{18,... | collective-permute-start | bytes 2162696 | tf_op jit(solution)/shard_map/ppermute | solution.py:16
  554.2 49.5 %collective-permute-start.8 = (bf16[2816,128]{1,0:T(8,128)(2,1)}, bf16[2816,128]{1,0:T(8,128)(2,1)S(1)}, u32[]{:S(2)}, u32[]{:S(2)}) collective-permute-start(bf16[2816,128]{1,0:T(8,128)(2,1)} %collective-permute-done.6), channel_id=1, source_target_pairs={{0,2},{2,4},{4,6},{6,8},{8,10},{10,12},{12,14},{14,16},{16,18},{18... | collective-permute-start | bytes 2162696 | tf_op jit(solution)/shard_map/ppermute | solution.py:13
  565.0 48.6 %collective-permute-start.9 = (bf16[2816,128]{1,0:T(8,128)(2,1)S(1)}, bf16[2816,128]{1,0:T(8,128)(2,1)S(1)}, u32[]{:S(2)}, u32[]{:S(2)}) collective-permute-start(bf16[2816,128]{1,0:T(8,128)(2,1)S(1)} %collective-permute-done.7), channel_id=1, source_target_pairs={{0,30},{2,0},{4,2},{6,4},{8,6},{10,8},{12,10},{14,12},{16,14},{18,... | collective-permute-start | bytes 2162696 | tf_op jit(solution)/shard_map/ppermute | solution.py:16
  603.7 41.0 %collective-permute-start.10 = (bf16[2816,128]{1,0:T(8,128)(2,1)S(1)}, bf16[2816,128]{1,0:T(8,128)(2,1)S(1)}, u32[]{:S(2)}, u32[]{:S(2)}) collective-permute-start(bf16[2816,128]{1,0:T(8,128)(2,1)S(1)} %collective-permute-done.8), channel_id=1, source_target_pairs={{0,2},{2,4},{4,6},{6,8},{8,10},{10,12},{12,14},{14,16},{16,18},{18... | collective-permute-start | bytes 2162696 | tf_op jit(solution)/shard_map/ppermute | solution.py:13
  613.6 35.5 %collective-permute-start.11 = (bf16[2816,128]{1,0:T(8,128)(2,1)S(1)}, bf16[2816,128]{1,0:T(8,128)(2,1)S(1)}, u32[]{:S(2)}, u32[]{:S(2)}) collective-permute-start(bf16[2816,128]{1,0:T(8,128)(2,1)S(1)} %collective-permute-done.9), channel_id=1, source_target_pairs={{0,30},{2,0},{4,2},{6,4},{8,6},{10,8},{12,10},{14,12},{16,14},{18,... | collective-permute-start | bytes 2162696 | tf_op jit(solution)/shard_map/ppermute | solution.py:16
  644.7 17.4 %collective-permute-start.12 = (bf16[2816,128]{1,0:T(8,128)(2,1)S(1)}, bf16[2816,128]{1,0:T(8,128)(2,1)S(1)}, u32[]{:S(2)}, u32[]{:S(2)}) collective-permute-start(bf16[2816,128]{1,0:T(8,128)(2,1)S(1)} %collective-permute-done.10), channel_id=1, source_target_pairs={{0,2},{2,4},{4,6},{6,8},{8,10},{10,12},{12,14},{14,16},{16,18},{18... | collective-permute-start | bytes 2162696 | tf_op jit(solution)/shard_map/ppermute | solution.py:13
  649.1 30.4 %collective-permute-start.13 = (bf16[2816,128]{1,0:T(8,128)(2,1)S(1)}, bf16[2816,128]{1,0:T(8,128)(2,1)S(1)}, u32[]{:S(2)}, u32[]{:S(2)}) collective-permute-start(bf16[2816,128]{1,0:T(8,128)(2,1)S(1)} %collective-permute-done.11), channel_id=1, source_target_pairs={{0,30},{2,0},{4,2},{6,4},{8,6},{10,8},{12,10},{14,12},{16,14},{18,... | collective-permute-start | bytes 2162696 | tf_op jit(solution)/shard_map/ppermute | solution.py:16
  662.0 30.9 %collective-permute-start.14 = (bf16[2816,128]{1,0:T(8,128)(2,1)S(1)}, bf16[2816,128]{1,0:T(8,128)(2,1)S(1)}, u32[]{:S(2)}, u32[]{:S(2)}) collective-permute-start(bf16[2816,128]{1,0:T(8,128)(2,1)S(1)} %collective-permute-done.12), channel_id=1, source_target_pairs={{0,2},{2,4},{4,6},{6,8},{8,10},{10,12},{12,14},{14,16},{16,18},{18... | collective-permute-start | bytes 2162696 | tf_op jit(solution)/shard_map/ppermute | solution.py:13
Sparse Core Ops, SparseCore 0:
  369.6 7.3 reduce-scatter.2
  381.4 11.8 all-gather.7
  396.0 235.5 all-gather.9
  634.3 180.4 all-gather.11
  838.2 7.9 reduce-scatter.4
